TPU v7x, 32 devices: a whole 2x2x4 slice. The times are simulated.
32 devices in a mesh: sp: 8 (over z, y), tp: 4 (over x, core).
Axes of the slice: x: 2, y: 2, z: 4, core: 2. Of those that a mesh axis runs over, the one named last changes fastest.
Arguments:
- queries: bfloat16 [1024, 1280], P('sp', 'tp'), may hold values from -4000 to 4000
- latents: bfloat16 [1024, 512], P('sp'), may hold values from -6 to 6
- shared_key: bfloat16 [1024, 64], P('sp'), may hold values from -4 to 4
- expand_weight: bfloat16 [512, 1536], P(None, 'tp'), may hold values from -0.25 to 0.25
- residual: bfloat16 [1024, 2048], P('sp'), may hold values from -3 to 3
- out_weight: bfloat16 [768, 2048], replicated, may hold values from -0.21875 to 0.21875
- norm_gain: bfloat16 [2048], replicated, may hold values from 0.099609375 to 1.8984375
- gate_weight: bfloat16 [2048, 3072], P('sp', 'tp'), may hold values from -0.125 to 0.125
- value_weight: bfloat16 [2048, 3072], P('sp', 'tp'), may hold values from -0.125 to 0.125
- conv_weight: bfloat16 [3, 3072], P(None, 'tp'), may hold values from -3.5 to 3.5
- down_weight: bfloat16 [3072, 2048], P('tp', 'sp'), may hold values from -0.109375 to 0.109375
Outputs:
- output: bfloat16 [1024, 2048], P(('sp', 'tp'))
All inputs are finite; a program needn't handle non-finite values.
Results may differ from a plain program's by a relative error of at most 0.018.
Values may be sent and summed in bfloat16 or wider, within the bound.
A program may use at most 128 MiB of HBM per device.

v0:
```python
import jax
import jax.numpy as jnp
from jax import lax
from jax.sharding import PartitionSpec as P

NOPE_A = 128
VAL_A = 128
NOPE_B = 64
VAL_B = 64
ROPE = 64


def padded_2(block, sides, width):
    for axis, dim in sides:
        count = lax.axis_size(axis)
        forward = [(i, i + 1) for i in range(count - 1)]
        backward = [(target, source) for source, target in forward]
        low = lax.ppermute(
            lax.slice_in_dim(block, block.shape[dim] - width, None, axis=dim), axis, forward
        )
        high = lax.ppermute(lax.slice_in_dim(block, 0, width, axis=dim), axis, backward)
        block = jnp.concatenate([low, block, high], axis=dim)
    return block


def tables(positions, width):
    half_width = width // 2
    frequency = 10000.0 ** (-jnp.arange(half_width, dtype=jnp.float32) / half_width)
    angles = positions.astype(jnp.float32)[:, None] * frequency[None, :]
    return (jnp.cos(angles), jnp.sin(angles))


def rotate(vectors, cos_table, sine_table):
    half_width = vectors.shape[-1] // 2
    first_half = vectors[:, :half_width].astype(jnp.float32)
    second_half = vectors[:, half_width:].astype(jnp.float32)
    turned = jnp.concatenate(
        [
            first_half * cos_table - second_half * sine_table,
            second_half * cos_table + first_half * sine_table,
        ],
        axis=1,
    )
    return turned.astype(jnp.bfloat16)


def normalize(stream, norm_gain):
    stream_f = stream.astype(jnp.float32)
    scaled = stream_f * lax.rsqrt(jnp.mean(stream_f * stream_f, axis=1, keepdims=True) + 1e-06)
    return (scaled * norm_gain.astype(jnp.float32)).astype(jnp.bfloat16)


def update(running, q_content, q_turned, k_content, k_turned, values, score_scale):
    row_max, row_sum, weighted = running
    scores = (
        jnp.einsum("qd,kd->qk", q_content, k_content, preferred_element_type=jnp.float32)
        + jnp.einsum("qd,kd->qk", q_turned, k_turned, preferred_element_type=jnp.float32)
    ) * score_scale
    new_max = jnp.maximum(row_max, jnp.max(scores, axis=1))
    weights = jnp.exp(scores - new_max[:, None])
    row_sum = jnp.sum(weights, axis=1)
    weighted = jnp.dot(weights.astype(jnp.bfloat16), values, preferred_element_type=jnp.float32)
    return (new_max, row_sum, weighted)


def body(
    queries,
    latents,
    shared_key,
    expand_weight,
    residual,
    out_weight,
    norm_gain,
    gate_weight,
    value_weight,
    conv_weight,
    down_weight,
):
    tok_rows = queries.shape[0]
    q_width = NOPE_A + NOPE_B + 2 * ROPE
    kv_width = NOPE_A + VAL_A + NOPE_B + VAL_B
    positions = lax.axis_index("sp") * tok_rows + jnp.arange(tok_rows, dtype=jnp.int32)
    cos_table, sine_table = tables(positions, ROPE)
    key_turned = rotate(shared_key, cos_table, sine_table)
    scale_wide = (NOPE_A + ROPE) ** (-0.5)
    scale_narrow = (NOPE_B + ROPE) ** (-0.5)
    initial = []
    pair_index = 0
    q_base = pair_index * q_width
    rotary_base = q_base + NOPE_A + NOPE_B
    wide_content = queries[:, q_base : q_base + NOPE_A]
    narrow_content = queries[:, q_base + NOPE_A : rotary_base]
    wide_turned = rotate(queries[:, rotary_base : rotary_base + ROPE], cos_table, sine_table)
    narrow_turned = rotate(
        queries[:, rotary_base + ROPE : rotary_base + 2 * ROPE], cos_table, sine_table
    )
    query_parts = [(wide_content, wide_turned, narrow_content, narrow_turned)]
    lowest = jnp.full((tok_rows,), -1e30, jnp.float32)
    empty_sum = jnp.zeros((tok_rows,), jnp.float32)
    initial += [
        lowest,
        empty_sum,
        jnp.zeros((tok_rows, VAL_A), jnp.float32),
        lowest,
        empty_sum,
        jnp.zeros((tok_rows, VAL_B), jnp.float32),
    ]
    initial = tuple(initial)
    pieces = (
        lax.all_gather(latents, "sp", axis=0, tiled=True),
        lax.all_gather(key_turned, "sp", axis=0, tiled=True),
    )
    expanded = jnp.dot(pieces[0], expand_weight, preferred_element_type=jnp.float32).astype(
        jnp.bfloat16
    )
    turned_keys = pieces[1]
    result = []
    pair_index = 0
    wide_content, wide_turned, narrow_content, narrow_turned = query_parts[pair_index]
    kv_base = pair_index * kv_width
    narrow_base = kv_base + NOPE_A + VAL_A
    wide_keys = expanded[:, kv_base : kv_base + NOPE_A]
    wide_values = expanded[:, kv_base + NOPE_A : narrow_base]
    narrow_keys = expanded[:, narrow_base : narrow_base + NOPE_B]
    narrow_values = expanded[:, narrow_base + NOPE_B : narrow_base + NOPE_B + VAL_B]
    absorb_offset = 6 * pair_index
    result += list(
        update(
            initial[absorb_offset : absorb_offset + 3],
            wide_content,
            wide_turned,
            wide_keys,
            turned_keys,
            wide_values,
            scale_wide,
        )
    )
    result += list(
        update(
            initial[absorb_offset + 3 : absorb_offset + 6],
            narrow_content,
            narrow_turned,
            narrow_keys,
            turned_keys,
            narrow_values,
            scale_narrow,
        )
    )
    running = tuple(result)
    outputs = []
    pair_index = 0
    for group_index in range(2):
        offset = 6 * pair_index + 3 * group_index
        outputs.append((running[offset + 2] / running[offset + 1][:, None]).astype(jnp.bfloat16))
    attended = jnp.concatenate(outputs, axis=1)
    share = tok_rows // lax.axis_size("tp")
    tp_index = lax.axis_index("tp")
    all_heads = lax.all_gather(attended, "tp", axis=1, tiled=True)
    projected = jnp.dot(all_heads, out_weight, preferred_element_type=jnp.float32)
    stream = (residual.astype(jnp.float32) + projected).astype(jnp.bfloat16)
    normed = normalize(stream, norm_gain)
    stream_own = lax.dynamic_slice_in_dim(stream, tp_index * share, share, 0)
    pieces = (
        lax.all_gather(gate_weight, "sp", axis=0, tiled=True),
        lax.all_gather(value_weight, "sp", axis=0, tiled=True),
    )
    gate_sum = jnp.dot(normed, pieces[0], preferred_element_type=jnp.float32)
    value_sum = jnp.dot(normed, pieces[1], preferred_element_type=jnp.float32)
    gate_pre = gate_sum.astype(jnp.bfloat16)
    value_pre = value_sum.astype(jnp.bfloat16)
    reach = conv_weight.shape[0] // 2
    padded = padded_2(gate_pre, (("sp", 0),), reach)
    mixed_gate = jnp.zeros(gate_pre.shape, jnp.float32)
    for tap in range(conv_weight.shape[0]):
        mixed_gate = mixed_gate + padded[tap : tap + tok_rows].astype(jnp.float32) * conv_weight[
            tap
        ].astype(jnp.float32)
    active = (jax.nn.silu(mixed_gate) * value_pre.astype(jnp.float32)).astype(jnp.bfloat16)
    partial_rows = jnp.dot(
        active,
        lax.all_gather(down_weight, "sp", axis=1, tiled=True),
        preferred_element_type=jnp.float32,
    )
    summed = lax.psum_scatter(
        partial_rows.astype(jnp.bfloat16), "tp", scatter_dimension=0, tiled=True
    ).astype(jnp.float32)
    return (stream_own.astype(jnp.float32) + summed).astype(jnp.bfloat16)


def solution(mesh):
    in_specs = (
        P("sp", "tp"),
        P("sp", None),
        P("sp", None),
        P(None, "tp"),
        P("sp", None),
        P(),
        P(),
        P("sp", "tp"),
        P("sp", "tp"),
        P(None, "tp"),
        P("tp", "sp"),
    )
    out_specs = P(("sp", "tp"), None)
    return jax.shard_map(body, mesh=mesh, in_specs=in_specs, out_specs=out_specs, check_vma=False)
```

profile of v0, /device:TPU:0, one launch (start us, length us, event | category | flops | bytes accessed | tf_op | source)
XLA Modules:
  0.0 271.1 jit_solution(13108688686888295058)
XLA Ops:
  6.5 0.7 all-gather.5.cloned.1.call-update
  7.3 0.0 all-gather.7.cloned.1.call-start
  7.3 0.7 all-gather.7.cloned.1.call-update
  8.0 0.0 all-gather.11.cloned.1.call-start
  8.1 0.7 all-gather.11.cloned.1.call-update
  8.7 0.0 all-gather.9.cloned.1.call-start
  8.8 0.5 all-gather.9.cloned.1.call-update
  9.3 0.0 reduce-scatter.2.cloned.1.call-start
  9.4 0.7 convert_element_type.113
  10.1 0.9 fusion.59
  11.0 28.2 %all_gather.19 = bf16[1024,64]{0,1:T(8,128)(2,1)S(1)} all-gather(bf16[128,64]{0,1:T(8,128)(2,1)S(1)} %pad_maximum_fusion.5), channel_id=1, replica_groups=mesh['sp'=8,'tp'=4] {'sp'}, dimensions={0}, use_global_device_ids=true | all-gather | bytes 147456 | tf_op jit(solution)/shard_map/all_gather | solution.py:111
  39.2 13.5 %all-gather.5.cloned.1.call-done = bf16[1024,512]{1,0:T(8,128)(2,1)} async-done(((bf16[128,512]{1,0:T(8,128)(2,1)}), bf16[1024,512]{1,0:T(8,128)(2,1)}) %all-gather.5.cloned.1.call-update) | async-done | bytes 1048592 | tf_op jit(solution)/shard_map/all_gather | solution.py:110
  52.7 1.9 convolution_convert_fusion.1
  54.7 0.3 convolution_bitcast_fusion.1
  54.9 0.4 fusion.83
  55.3 0.2 fusion.11
  55.5 0.3 convolution_bitcast_fusion
  55.7 0.4 fusion.82
  56.1 0.2 fusion.13
  56.3 0.2 fusion.7
  56.5 0.3 fusion.6
  56.8 5.6 %all_gather.20 = bf16[128,768]{0,1:T(8,128)(2,1)S(1)} all-gather(bf16[128,192]{0,1:T(8,128)(2,1)S(1)} %pad_maximum_fusion.4), channel_id=1, replica_groups=mesh['sp'=8,'tp'=4] {'tp'}, dimensions={1}, use_global_device_ids=true | all-gather | bytes 245760 | tf_op jit(solution)/shard_map/all_gather | solution.py:158
  62.4 1.4 fusion.8
  63.8 49.9 %all-gather.7.cloned.1.call-done = bf16[2048,768]{1,0:T(8,128)(2,1)} async-done(((bf16[256,768]{1,0:T(8,128)(2,1)}), bf16[2048,768]{1,0:T(8,128)(2,1)}) %all-gather.7.cloned.1.call-update) | async-done | bytes 3145744 | tf_op jit(solution)/shard_map/all_gather | solution.py:164
  113.7 2.7 convolution_convert_fusion.3
  116.4 2.5 collective-permute-start
  118.8 1.3 collective-permute-start.1
  120.2 56.9 %all-gather.11.cloned.1.call-done = bf16[768,2048]{1,0:T(8,128)(2,1)} async-done(((bf16[768,256]{1,0:T(8,128)(2,1)}), bf16[768,2048]{1,0:T(8,128)(2,1)}) %all-gather.11.cloned.1.call-update) | async-done | bytes 3145744 | tf_op jit(solution)/shard_map/all_gather | solution.py:181
  177.1 60.3 %all-gather.9.cloned.1.call-done = bf16[2048,768]{1,0:T(8,128)(2,1)} async-done(((bf16[256,768]{1,0:T(8,128)(2,1)}), bf16[2048,768]{1,0:T(8,128)(2,1)}) %all-gather.9.cloned.1.call-update) | async-done | bytes 3145744 | tf_op jit(solution)/shard_map/all_gather | solution.py:165
  237.3 5.1 %convolution_convert_fusion = bf16[128,2048]{1,0:T(8,128)(2,1)} fusion(bf16[768,2048]{1,0:T(8,128)(2,1)} %all-gather.11.cloned.1.call-done, bf16[2048,768]{1,0:T(8,128)(2,1)} %all-gather.9.cloned.1.call-done, bf16[128,768]{1,0:T(8,128)(2,1)S(1)} %convolution_convert_fusion.3, bf16[1,768]{1,0:T(2,128)(2,1)S(1)} %collective-permute-done.1, ...), kind=kOutput, calls=%fused_computation.2 | convolution fusion | flops 808779776 | bytes 7557632 | tf_op jit(solution)/shard_map/dot_general | solution.py:179
  242.5 20.5 %reduce-scatter.2.cloned.1.call-done = bf16[32,2048]{1,0:T(8,128)(2,1)} async-done(((bf16[128,2048]{1,0:T(8,128)(2,1)}), bf16[32,2048]{1,0:T(8,128)(2,1)}) %reduce-scatter.2.cloned.1.call-update) | async-done | bytes 131088 | tf_op jit(solution)/shard_map/reduce_scatter | solution.py:184
  262.9 1.7 add_convert_fusion
  (21 shorter events, 0.1 us)
Async XLA Ops:
  6.5 55.8 %copy-start = (bf16[768,2048]{1,0:T(8,128)(2,1)S(1)}, bf16[768,2048]{1,0:T(8,128)(2,1)}, u32[]{:S(2)}) copy-start(bf16[768,2048]{1,0:T(8,128)(2,1)} %param.16) | copy-start | bytes 9437188
  6.5 48.1 %copy-start.2 = (bf16[128,320]{0,1:T(8,128)(2,1)S(1)}, bf16[128,320]{0,1:T(8,128)(2,1)}, u32[]{:S(2)}) copy-start(bf16[128,320]{0,1:T(8,128)(2,1)} %param.11) | copy-start | bytes 245764
  6.5 46.2 %all-gather.5.cloned.1.call-start = ((), (), s32[]{:S(2)}) async-start(), calls=%async_computation.1 | async-start | bytes 1179648 | tf_op jit(solution)/shard_map/all_gather | solution.py:110
  7.3 106.4 %all-gather.7.cloned.1.call-start = ((), (), s32[]{:S(2)}) async-start(), calls=%async_computation.2 | async-start | bytes 3538944 | tf_op jit(solution)/shard_map/all_gather | solution.py:164
  8.0 169.1 %all-gather.11.cloned.1.call-start = ((), (), s32[]{:S(2)}) async-start(), calls=%async_computation.4 | async-start | bytes 3538944 | tf_op jit(solution)/shard_map/all_gather | solution.py:181
  8.7 228.6 %all-gather.9.cloned.1.call-start = ((), (), s32[]{:S(2)}) async-start(), calls=%async_computation.3 | async-start | bytes 3538944 | tf_op jit(solution)/shard_map/all_gather | solution.py:165
  9.3 253.6 %reduce-scatter.2.cloned.1.call-start = ((), (), s32[]{:S(2)}) async-start(), calls=%async_computation.5 | async-start | bytes 655360 | tf_op jit(solution)/shard_map/reduce_scatter | solution.py:184
  54.9 7.4 %copy-start.1 = (bf16[128,2048]{1,0:T(8,128)(2,1)S(1)}, bf16[128,2048]{1,0:T(8,128)(2,1)}, u32[]{:S(2)}) copy-start(bf16[128,2048]{1,0:T(8,128)(2,1)} %param.15) | copy-start | bytes 1572868
  62.4 57.8 %copy-start.3 = (bf16[3,768]{1,0:T(4,128)(2,1)S(1)}, bf16[3,768]{1,0:T(4,128)(2,1)}, u32[]{:S(2)}) copy-start(bf16[3,768]{1,0:T(4,128)(2,1)} %param.20) | copy-start | bytes 13828
  116.4 121.0 %collective-permute-start = (bf16[1,768]{1,0:T(2,128)(2,1)S(1)}, bf16[1,768]{1,0:T(2,128)(2,1)S(1)}, u32[]{:S(2)}, u32[]{:S(2)}) collective-permute-start(bf16[1,768]{1,0:T(2,128)(2,1)S(1)} %get-tuple-element.8), channel_id=1, source_target_pairs={{0,4},{4,8},{8,12},{12,16},{16,20},{20,24},{24,28},{1,5},{5,9},{9,... | collective-permute-start | bytes 4616 | tf_op jit(solution)/shard_map/ppermute | solution.py:18
  118.8 118.5 %collective-permute-start.1 = (bf16[1,768]{1,0:T(2,128)(2,1)S(1)}, bf16[1,768]{1,0:T(2,128)(2,1)S(1)}, u32[]{:S(2)}, u32[]{:S(2)}) collective-permute-start(bf16[1,768]{1,0:T(2,128)(2,1)S(1)} %get-tuple-element.9), channel_id=1, source_target_pairs={{4,0},{8,4},{12,8},{16,12},{20,16},{24,20},{28,24},{5,1},{9,5},{13... | collective-permute-start | bytes 4616 | tf_op jit(solution)/shard_map/ppermute | solution.py:21
Sparse Core Ops, SparseCore 0:
  9.5 43.2 all-gather.4
  54.9 58.7 all-gather.6
  115.7 61.2 all-gather.10
  179.1 58.1 all-gather.8
  242.6 20.2 reduce-scatter.1
where the time goes:
time: 271 us
  waiting for transfers between devices  204 us (75%)
  blocking collectives  33.8 us (12%)
  between operations  13.3 us (5%)
  matrix products  12.8 us (5%)
  starting transfers between devices  3.9 us (1%)
  other arithmetic  3.68 us (1%)
    all_gather x1, waiting for transfers between devices, body(): lax.all_gather(value_weight, 'sp', axis=0, tiled=True)  60.3 us
    all_gather x1, waiting for transfers between devices, body(): lax.all_gather(down_weight, 'sp', axis=1, tiled=True)  56.9 us
    all_gather x1, waiting for transfers between devices, body(): lax.all_gather(gate_weight, 'sp', axis=0, tiled=True)  49.9 us
    all_gather x1, blocking collectives, body(): lax.all_gather(key_turned, 'sp', axis=0, tiled=True)  28.2 us
    reduce_scatter x1, waiting for transfers between devices, body(): lax.psum_scatter(partial_rows.astype(jnp.bfloat16), 'tp', scatter_dimensi...  20.5 us
    all_gather x1, waiting for transfers between devices, body(): lax.all_gather(latents, 'sp', axis=0, tiled=True)  13.5 us
    all_gather x1, blocking collectives, body(): all_heads = lax.all_gather(attended, 'tp', axis=1, tiled=True)  5.6 us
  transfers between devices with their start and end apart: 7, of which 5 were waited for; matrix products, arithmetic and copies ran while one was open for 4% of the time, Pallas kernels for 0%

commit v1 on v0

--- a/solution.py
+++ b/solution.py
@@ -8,6 +8,13 @@
 NOPE_B = 64
 VAL_B = 64
 ROPE = 64
+
+
+def swapped_in(shard, name, dim):
+    count = lax.axis_size(name)
+    pieces = jnp.stack([shard for _ in range(count)])
+    pieces = lax.all_to_all(pieces, name, split_axis=0, concat_axis=0)
+    return jnp.concatenate(pieces, axis=dim)
 
 
 def padded_2(block, sides, width):
@@ -161,7 +168,7 @@
     normed = normalize(stream, norm_gain)
     stream_own = lax.dynamic_slice_in_dim(stream, tp_index * share, share, 0)
     pieces = (
-        lax.all_gather(gate_weight, "sp", axis=0, tiled=True),
+        swapped_in(gate_weight, "sp", 0),
         lax.all_gather(value_weight, "sp", axis=0, tiled=True),
     )
     gate_sum = jnp.dot(normed, pieces[0], preferred_element_type=jnp.float32)

time: 271 us -> 259 us (0.956)
  waiting for transfers between devices: 204 us -> 110 us
  blocking collectives: 33.8 us -> 107 us
  starting transfers between devices: 3.9 us -> 10.1 us
  local copies, waits for them, and re-layouts: 0.03 us -> 2.87 us
    all_gather x1, blocking collectives: 28.2 us -> 102 us  [body(): lax.all_gather(key_turned, 'sp', axis=0, tiled=True)]
    all_gather x1 -> x0, waiting for transfers between devices: 49.9 us -> none  [body(): lax.all_gather(gate_weight, 'sp', axis=0, tiled=True)]
    all_gather x1, waiting for transfers between devices: 60.3 us -> 24.7 us  [body(): lax.all_gather(value_weight, 'sp', axis=0, tiled=True)]
    all_gather x1, waiting for transfers between devices: 13.5 us -> 0.01 us  [body(): lax.all_gather(latents, 'sp', axis=0, tiled=True)]
    all_to_all x0 -> x1, starting transfers between devices: none -> 7.44 us  [swapped_in(): pieces = lax.all_to_all(pieces, name, split_axis=0, concat_axis=0)]
    all_gather x1, waiting for transfers between devices: 56.9 us -> 63.4 us  [body(): lax.all_gather(down_weight, 'sp', axis=1, tiled=True)]
    another operation x0 -> x1, local copies, waits for them, and re-layouts: none -> 2.84 us  [swapped_in(): pieces = jnp.stack([shard for _ in range(count)])]
  transfers between devices with their start and end apart: 7 -> 7, of which waited for: 5 -> 3; matrix products, arithmetic and copies ran while one was open for 4% -> 4% of each run, Pallas kernels for 0% -> 0%
where the time goes in v1:
time: 259 us
  waiting for transfers between devices  110 us (42%)
  blocking collectives  107 us (41%)
  between operations  13.3 us (5%)
  matrix products  12.9 us (5%)
  starting transfers between devices  10.1 us (4%)
  local copies, waits for them, and re-layouts  2.87 us (1%)
    all_gather x1, blocking collectives, body(): lax.all_gather(key_turned, 'sp', axis=0, tiled=True)  102 us
    all_gather x1, waiting for transfers between devices, body(): lax.all_gather(down_weight, 'sp', axis=1, tiled=True)  63.4 us
    all_gather x1, waiting for transfers between devices, body(): lax.all_gather(value_weight, 'sp', axis=0, tiled=True)  24.7 us
    reduce_scatter x1, waiting for transfers between devices, body(): lax.psum_scatter(partial_rows.astype(jnp.bfloat16), 'tp', scatter_dimensi...  20 us
    all_to_all x1, starting transfers between devices, swapped_in(): pieces = lax.all_to_all(pieces, name, split_axis=0, concat_axis=0)  7.44 us
    all_gather x1, blocking collectives, body(): all_heads = lax.all_gather(attended, 'tp', axis=1, tiled=True)  5.6 us
  transfers between devices with their start and end apart: 7, of which 3 were waited for; matrix products, arithmetic and copies ran while one was open for 4% of the time, Pallas kernels for 0%

profile of v1, /device:TPU:0, one launch (start us, length us, event | category | flops | bytes accessed | tf_op | source)
XLA Modules:
  0.0 259.0 jit_solution(6528066936536387348)
XLA Ops:
  6.5 0.7 all-gather.4.cloned.1.call-update
  7.3 0.0 all-gather.6.cloned.1.call-start
  7.3 0.7 all-gather.6.cloned.1.call-update
  8.0 2.8 %stack.2 = bf16[8,256,768]{2,1,0:T(8,128)(2,1)} broadcast(bf16[256,768]{1,0:T(8,128)(2,1)} %param.18), dimensions={1,2} | broadcast | bytes 3538944 | tf_op jit(solution)/shard_map/stack | solution.py:15
  10.9 7.4 %all-to-all-start = ((bf16[8,256,768]{2,1,0:T(8,128)(2,1)}), bf16[8,256,768]{2,1,0:T(8,128)(2,1)}, u32[]{:S(2)}, u32[]{:S(2)}) async-start(bf16[8,256,768]{2,1,0:T(8,128)(2,1)} %stack.2), calls=%async_computation | async-start | bytes 6291456 | tf_op jit(solution)/shard_map/all_to_all | solution.py:16
  18.3 0.0 all-gather.8.cloned.1.call-start
  18.3 0.7 all-gather.8.cloned.1.call-update
  19.0 0.0 reduce-scatter.2.cloned.1.call-start
  19.1 0.2 fusion.59
  19.3 101.8 %all_gather.16 = bf16[1024,64]{0,1:T(8,128)(2,1)S(1)} all-gather(bf16[128,64]{0,1:T(8,128)(2,1)S(1)} %pad_maximum_fusion.5), channel_id=1, replica_groups=mesh['sp'=8,'tp'=4] {'sp'}, dimensions={0}, use_global_device_ids=true | all-gather | bytes 147456 | tf_op jit(solution)/shard_map/all_gather | solution.py:118
  121.1 1.9 convolution_convert_fusion.1
  123.1 0.3 convolution_bitcast_fusion.1
  123.3 0.0 copy-start.1
  123.3 0.4 fusion.83
  123.7 0.2 fusion.11
  123.9 0.3 convolution_bitcast_fusion
  124.1 0.4 fusion.82
  124.5 0.2 fusion.13
  124.6 0.2 fusion.7
  124.9 0.3 fusion.6
  125.2 5.6 %all_gather.17 = bf16[128,768]{0,1:T(8,128)(2,1)S(1)} all-gather(bf16[128,192]{0,1:T(8,128)(2,1)S(1)} %pad_maximum_fusion.4), channel_id=1, replica_groups=mesh['sp'=8,'tp'=4] {'tp'}, dimensions={1}, use_global_device_ids=true | all-gather | bytes 245760 | tf_op jit(solution)/shard_map/all_gather | solution.py:165
  130.8 1.5 fusion.8
  132.2 2.7 %convolution_convert_fusion.3 = bf16[128,768]{1,0:T(8,128)(2,1)S(1)} fusion(bf16[2048,768]{1,0:T(8,128)(2,1)} %bitcast.2, bf16[128,2048]{1,0:T(8,128)(2,1)} %get-tuple-element.23, f32[2048]{0:T(1024)S(1)} %convert_element_type.113, f32[128]{0:T(128)S(1)} %add_rsqrt_fusion), kind=kOutput, calls=%fused_computation.16 | convolution fusion | flops 403800064 | bytes 3875328 | tf_op jit(solution)/shard_map/dot_general | solution.py:174
  134.9 1.3 collective-permute-start
  136.2 1.3 collective-permute-start.1
  137.6 24.7 %all-gather.6.cloned.1.call-done = bf16[2048,768]{1,0:T(8,128)(2,1)} async-done(((bf16[256,768]{1,0:T(8,128)(2,1)}), bf16[2048,768]{1,0:T(8,128)(2,1)}) %all-gather.6.cloned.1.call-update) | async-done | bytes 3145744 | tf_op jit(solution)/shard_map/all_gather | solution.py:172
  162.3 63.4 %all-gather.8.cloned.1.call-done = bf16[768,2048]{1,0:T(8,128)(2,1)} async-done(((bf16[768,256]{1,0:T(8,128)(2,1)}), bf16[768,2048]{1,0:T(8,128)(2,1)}) %all-gather.8.cloned.1.call-update) | async-done | bytes 3145744 | tf_op jit(solution)/shard_map/all_gather | solution.py:188
  225.7 0.0 collective-permute-done
  225.7 5.1 %convolution_convert_fusion = bf16[128,2048]{1,0:T(8,128)(2,1)} fusion(bf16[768,2048]{1,0:T(8,128)(2,1)} %all-gather.8.cloned.1.call-done, bf16[2048,768]{1,0:T(8,128)(2,1)} %all-gather.6.cloned.1.call-done, bf16[128,768]{1,0:T(8,128)(2,1)S(1)} %convolution_convert_fusion.3, bf16[1,768]{1,0:T(2,128)(2,1)S(1)} %collective-permute-done.1, ...), kind=kOutput, calls=%fused_computation.2 | convolution fusion | flops 808779776 | bytes 7557632 | tf_op jit(solution)/shard_map/dot_general | solution.py:186
  230.8 0.0 reduce-scatter.2.cloned.1.call-update
  230.9 20.0 %reduce-scatter.2.cloned.1.call-done = bf16[32,2048]{1,0:T(8,128)(2,1)} async-done(((bf16[128,2048]{1,0:T(8,128)(2,1)}), bf16[32,2048]{1,0:T(8,128)(2,1)}) %reduce-scatter.2.cloned.1.call-update) | async-done | bytes 131088 | tf_op jit(solution)/shard_map/reduce_scatter | solution.py:191
  250.9 1.7 add_convert_fusion
  (25 shorter events, 0.1 us)
Async XLA Ops:
  6.5 124.2 %copy-start = (bf16[768,2048]{1,0:T(8,128)(2,1)S(1)}, bf16[768,2048]{1,0:T(8,128)(2,1)}, u32[]{:S(2)}) copy-start(bf16[768,2048]{1,0:T(8,128)(2,1)} %param.16) | copy-start | bytes 9437188
  6.5 114.6 %all-gather.4.cloned.1.call-start = ((), (), s32[]{:S(2)}) async-start(), calls=%async_computation.2 | async-start | bytes 1179648 | tf_op jit(solution)/shard_map/all_gather | solution.py:117
  7.3 155.1 %all-gather.6.cloned.1.call-start = ((), (), s32[]{:S(2)}) async-start(), calls=%async_computation.3 | async-start | bytes 3538944 | tf_op jit(solution)/shard_map/all_gather | solution.py:172
  10.8 8.2 %copy-start.5 = (bf16[2048]{0:T(1024)(128)(2,1)S(1)}, bf16[2048]{0:T(1024)(128)(2,1)}, u32[]{:S(2)}) copy-start(bf16[2048]{0:T(1024)(128)(2,1)} %param.17) | copy-start | bytes 12292
  10.8 8.3 %copy-start.2 = (bf16[128,320]{0,1:T(8,128)(2,1)S(1)}, bf16[128,320]{0,1:T(8,128)(2,1)}, u32[]{:S(2)}) copy-start(bf16[128,320]{0,1:T(8,128)(2,1)} %param.11) | copy-start | bytes 245764
  10.9 8.3 %copy-start.3 = (bf16[128,64]{0,1:T(8,128)(2,1)S(1)}, bf16[128,64]{0,1:T(8,128)(2,1)}, u32[]{:S(2)}) copy-start(bf16[128,64]{0,1:T(8,128)(2,1)} %param.13) | copy-start | bytes 49156
  10.9 121.4 %all-to-all-start = ((bf16[8,256,768]{2,1,0:T(8,128)(2,1)}), bf16[8,256,768]{2,1,0:T(8,128)(2,1)}, u32[]{:S(2)}, u32[]{:S(2)}) async-start(bf16[8,256,768]{2,1,0:T(8,128)(2,1)} %stack.2), calls=%async_computation | async-start | bytes 6291456 | tf_op jit(solution)/shard_map/all_to_all | solution.py:16
  18.3 207.4 %all-gather.8.cloned.1.call-start = ((), (), s32[]{:S(2)}) async-start(), calls=%async_computation.4 | async-start | bytes 3538944 | tf_op jit(solution)/shard_map/all_gather | solution.py:188
  19.0 231.8 %reduce-scatter.2.cloned.1.call-start = ((), (), s32[]{:S(2)}) async-start(), calls=%async_computation.5 | async-start | bytes 655360 | tf_op jit(solution)/shard_map/reduce_scatter | solution.py:191
  123.3 7.4 %copy-start.1 = (bf16[128,2048]{1,0:T(8,128)(2,1)S(1)}, bf16[128,2048]{1,0:T(8,128)(2,1)}, u32[]{:S(2)}) copy-start(bf16[128,2048]{1,0:T(8,128)(2,1)} %param.15) | copy-start | bytes 1572868
  130.8 6.8 %copy-start.4 = (bf16[3,768]{1,0:T(4,128)(2,1)S(1)}, bf16[3,768]{1,0:T(4,128)(2,1)}, u32[]{:S(2)}) copy-start(bf16[3,768]{1,0:T(4,128)(2,1)} %param.20) | copy-start | bytes 13828
  134.9 90.8 %collective-permute-start = (bf16[1,768]{1,0:T(2,128)(2,1)S(1)}, bf16[1,768]{1,0:T(2,128)(2,1)S(1)}, u32[]{:S(2)}, u32[]{:S(2)}) collective-permute-start(bf16[1,768]{1,0:T(2,128)(2,1)S(1)} %get-tuple-element.8), channel_id=1, source_target_pairs={{0,4},{4,8},{8,12},{12,16},{16,20},{20,24},{24,28},{1,5},{5,9},{9,... | collective-permute-start | bytes 4616 | tf_op jit(solution)/shard_map/ppermute | solution.py:25
  136.2 89.5 %collective-permute-start.1 = (bf16[1,768]{1,0:T(2,128)(2,1)S(1)}, bf16[1,768]{1,0:T(2,128)(2,1)S(1)}, u32[]{:S(2)}, u32[]{:S(2)}) collective-permute-start(bf16[1,768]{1,0:T(2,128)(2,1)S(1)} %get-tuple-element.9), channel_id=1, source_target_pairs={{4,0},{8,4},{12,8},{16,12},{20,16},{24,20},{28,24},{5,1},{9,5},{13... | collective-permute-start | bytes 4616 | tf_op jit(solution)/shard_map/ppermute | solution.py:28
Sparse Core Ops, SparseCore 0:
  9.5 92.8 all-gather.3
  104.5 57.7 all-gather.5
  164.4 61.3 all-gather.7
  231.0 19.8 reduce-scatter.1
